TPU v7x, 32 devices: a whole 2x2x4 slice. The times are simulated.
32 devices in a mesh: grp: 2 (over y), fs: 4 (over z), tp: 4 (over x, core).
Axes of the slice: x: 2, y: 2, z: 4, core: 2. Of those that a mesh axis runs over, the one named last changes fastest.
Arguments:
- tokens: bfloat16 [8, 384, 2048], P(('grp', 'fs'), None, 'tp'), parts along dimension 0, may hold values from -24 to 24
- input_gain: float32 [2048], replicated, may hold values from 0.1 to 1.9
- query_weight: bfloat16 [2048, 1024], P('fs', 'tp'), may hold values from -0.125 to 0.125
- key_weight: bfloat16 [2048, 1024], P('fs', 'tp'), may hold values from -0.125 to 0.125
- value_weight: bfloat16 [2048, 1024], P('fs', 'tp'), may hold values from -0.125 to 0.125
- output_gate_matrix: bfloat16 [2048, 1024], P('fs', 'tp'), may hold values from -0.125 to 0.125
- forward_decay: float32 [16], P('tp'), may hold values from -1 to 9
- backward_decay: float32 [16], P('tp'), may hold values from -1 to 9
- merge_weight: bfloat16 [1024, 2048], P('tp', 'fs'), may hold values from -0.375 to 0.375
- middle_gain: float32 [2048], replicated, may hold values from 0.1 to 1.9
- gate_weight: bfloat16 [2048, 5120], P('fs', 'tp'), may hold values from -0.125 to 0.125
- up_weight: bfloat16 [2048, 5120], P('fs', 'tp'), may hold values from -0.125 to 0.125
- down_weight: bfloat16 [5120, 2048], P('tp', 'fs'), may hold values from -0.15625 to 0.15625
Outputs:
- layer_out: bfloat16 [8, 384, 2048], P(('grp', 'fs'), None, 'tp'), parts along dimension 0
There are 2 independent parts, one for each index of `grp`. A program takes and returns all parts, laid end to end along the dimension named above; an argument that names none is the same for every part. Nothing has to cross between parts.
All inputs are finite; a program needn't handle non-finite values.
Results may differ from a plain program's by a relative error of at most 0.019.
Values may be sent and summed in bfloat16 or wider, within the bound.
A program may use at most 64 MiB of HBM per device.

v0:
```python
import jax
import jax.numpy as jnp
from jax import lax
from jax.sharding import PartitionSpec as P

BLOCK = 128
norm_eps = 1e-06
group_eps = 1e-05
rope_base = 10000.0
highest_precision = lax.Precision.HIGHEST


def rms_scale(values, gain_vector):
    widened = values.astype(jnp.float32)
    scaled = widened * lax.rsqrt(jnp.mean(widened * widened, axis=-1, keepdims=True) + norm_eps)
    return (scaled * gain_vector).astype(jnp.bfloat16)


def apply_rotary_heads(values, length):
    half_dim = values.shape[-1] // 2
    inverse = rope_base ** (-jnp.arange(half_dim, dtype=jnp.float32) / half_dim)
    angles = jnp.arange(length, dtype=jnp.float32)[:, None] * inverse[None, :]
    cosine = jnp.cos(angles)[:, None, :]
    sine_part = jnp.sin(angles)[:, None, :]
    lower_half = values[..., :half_dim]
    upper_half = values[..., half_dim:]
    return jnp.concatenate(
        [
            lower_half * cosine - upper_half * sine_part,
            upper_half * cosine + lower_half * sine_part,
        ],
        axis=-1,
    )


def carry_states(key_blocks, value_blocks, weighting, log_rates, block_size, backward):
    block_terms = jnp.einsum(
        "sbmhd,sbmhe->bshde",
        key_blocks * weighting[None, None, :, :, None],
        value_blocks,
        precision=highest_precision,
    )
    factor = jnp.exp(log_rates * block_size)[None, :, None, None]

    def advance(running, addend):
        return (running * factor + addend, running)

    initial = jnp.zeros(block_terms.shape[1:], jnp.float32)
    return lax.scan(advance, initial, block_terms, reverse=backward)[1]


def retain_blocks(
    query_rows, key_rows, value_rows, gate_rows, forward_decay, backward_decay, seq_count, length
):
    head_count = forward_decay.shape[0]
    head_dim = query_rows.shape[1] // head_count
    block_size = BLOCK
    block_count = length // block_size

    def split_heads(rows_in):
        return rows_in.astype(jnp.float32).reshape(seq_count, length, head_count, head_dim)

    def blocked(tensor):
        return tensor.reshape(seq_count, block_count, block_size, head_count, head_dim)

    queries = blocked(apply_rotary_heads(split_heads(query_rows), length))
    key_heads = blocked(apply_rotary_heads(split_heads(key_rows), length) * head_dim ** (-0.5))
    valued = blocked(split_heads(value_rows))
    rate_ahead = jax.nn.log_sigmoid(forward_decay)
    rate_behind = jax.nn.log_sigmoid(backward_decay)
    position = jnp.arange(block_size, dtype=jnp.float32)
    offset = position[:, None] - position[None, :]
    inside = jnp.where(
        offset[None] >= 0,
        jnp.exp(rate_ahead[:, None, None] * jnp.maximum(offset, 0.0)[None]),
        jnp.exp(rate_behind[:, None, None] * jnp.maximum(-offset, 0.0)[None]),
    )
    attention_scores = (
        jnp.einsum("sbchd,sbmhd->sbhcm", queries, key_heads, precision=highest_precision)
        * inside[None, None]
    )
    result = jnp.einsum("sbhcm,sbmhd->sbchd", attention_scores, valued, precision=highest_precision)
    column = position[:, None]
    key_ahead = jnp.exp(rate_ahead[None, :] * (block_size - 1 - column))
    query_ahead = jnp.exp(rate_ahead[None, :] * (column + 1))
    key_behind = jnp.exp(rate_behind[None, :] * column)
    query_behind = jnp.exp(rate_behind[None, :] * (block_size - column))
    from_before = carry_states(key_heads, valued, key_ahead, rate_ahead, block_size, False)
    from_after = carry_states(key_heads, valued, key_behind, rate_behind, block_size, True)
    result = (
        result
        + jnp.einsum("sbchd,bshde->sbche", queries, from_before, precision=highest_precision)
        * query_ahead[None, None, :, :, None]
    )
    result = (
        result
        + jnp.einsum("sbchd,bshde->sbche", queries, from_after, precision=highest_precision)
        * query_behind[None, None, :, :, None]
    )
    result = result.reshape(seq_count, length, head_count, head_dim)
    center = jnp.mean(result, axis=-1, keepdims=True)
    spread = jnp.mean(jnp.square(result - center), axis=-1, keepdims=True)
    normalized = (result - center) * lax.rsqrt(spread + group_eps)
    gated = jax.nn.silu(split_heads(gate_rows)) * normalized
    return gated.reshape(seq_count * length, head_count * head_dim).astype(jnp.bfloat16)


def accumulate(pieces, source):
    return tuple(
        (
            jnp.dot(source, weight_piece, preferred_element_type=jnp.float32)
            for weight_piece in pieces
        )
    )


def on_device(
    tokens,
    input_gain,
    query_weight,
    key_weight,
    value_weight,
    output_gate_matrix,
    forward_decay,
    backward_decay,
    merge_weight,
    middle_gain,
    gate_weight,
    up_weight,
    down_weight,
):
    seq_count, length, part_width = tokens.shape
    row_count = seq_count * length
    gathered = lax.all_gather(tokens, "tp", axis=2, tiled=True)
    normed = rms_scale(gathered.reshape(row_count, gathered.shape[2]), input_gain)
    query_sum, key_sum, value_sum, gating_sum = accumulate(
        (
            lax.all_gather(query_weight, "fs", axis=0, tiled=True),
            lax.all_gather(key_weight, "fs", axis=0, tiled=True),
            lax.all_gather(value_weight, "fs", axis=0, tiled=True),
            lax.all_gather(output_gate_matrix, "fs", axis=0, tiled=True),
        ),
        normed,
    )
    mixed = retain_blocks(
        query_sum.astype(jnp.bfloat16),
        key_sum.astype(jnp.bfloat16),
        value_sum.astype(jnp.bfloat16),
        gating_sum.astype(jnp.bfloat16),
        forward_decay,
        backward_decay,
        seq_count,
        length,
    )
    merge_term = jnp.dot(
        mixed,
        lax.all_gather(merge_weight, "fs", axis=1, tiled=True),
        preferred_element_type=jnp.float32,
    )
    merged = lax.psum_scatter(
        merge_term.astype(jnp.bfloat16), "tp", scatter_dimension=1, tiled=True
    ).astype(jnp.float32)
    middle = (tokens.reshape(row_count, part_width).astype(jnp.float32) + merged).astype(
        jnp.bfloat16
    )
    gathered_mid = lax.all_gather(middle, "tp", axis=1, tiled=True)
    normed_mid = rms_scale(gathered_mid, middle_gain)
    gate_full, up_full = (
        lax.all_gather(gate_weight, "fs", axis=0, tiled=True),
        lax.all_gather(up_weight, "fs", axis=0, tiled=True),
    )
    gate_act = jnp.dot(normed_mid, gate_full, preferred_element_type=jnp.float32)
    up_act = jnp.dot(normed_mid, up_full, preferred_element_type=jnp.float32)
    hidden = (jax.nn.silu(gate_act) * up_act).astype(jnp.bfloat16)
    down_term = jnp.dot(
        hidden,
        lax.all_gather(down_weight, "fs", axis=1, tiled=True),
        preferred_element_type=jnp.float32,
    )
    summed = lax.psum_scatter(
        down_term.astype(jnp.bfloat16), "tp", scatter_dimension=1, tiled=True
    ).astype(jnp.float32)
    layer_out = (middle.astype(jnp.float32) + summed).astype(jnp.bfloat16)
    return layer_out.reshape(seq_count, length, part_width)


def solution(mesh):
    placed = (
        P(("grp", "fs"), None, "tp"),
        P(),
        P("fs", "tp"),
        P("fs", "tp"),
        P("fs", "tp"),
        P("fs", "tp"),
        P("tp"),
        P("tp"),
        P("tp", "fs"),
        P(),
        P("fs", "tp"),
        P("fs", "tp"),
        P("tp", "fs"),
    )
    return jax.shard_map(
        on_device,
        mesh=mesh,
        in_specs=placed,
        out_specs=P(("grp", "fs"), None, "tp"),
        check_vma=False,
    )
```

profile of v0, /device:TPU:0, one launch (start us, length us, event | category | flops | bytes accessed | tf_op | source)
XLA Modules:
  0.0 571.5 jit_solution(758774433648440747)
XLA Ops:
  6.5 0.7 all-gather.11.cloned.1.call-update
  13.1 18.2 %all-gather.11.cloned.1.call-done = bf16[1,384,2048]{2,1,0:T(8,128)(2,1)} async-done(((bf16[1,384,512]{2,1,0:T(8,128)(2,1)}), bf16[1,384,2048]{2,1,0:T(8,128)(2,1)}) %all-gather.11.cloned.1.call-update) | async-done | bytes 1572880 | tf_op jit(solution)/shard_map/all_gather | solution.py:134
  31.3 1.9 fusion.3
  33.2 27.7 %all-gather.17.cloned.1.call-done = bf16[2048,256]{1,0:T(8,128)(2,1)} async-done(((bf16[512,256]{1,0:T(8,128)(2,1)}), bf16[2048,256]{1,0:T(8,128)(2,1)}) %all-gather.17.cloned.1.call-update) | async-done | bytes 1048592 | tf_op jit(solution)/shard_map/all_gather | solution.py:138
  60.9 2.6 convolution_convert_fusion.3
  63.5 26.4 %all-gather.19.cloned.1.call-done = bf16[2048,256]{1,0:T(8,128)(2,1)} async-done(((bf16[512,256]{1,0:T(8,128)(2,1)}), bf16[2048,256]{1,0:T(8,128)(2,1)}) %all-gather.19.cloned.1.call-update) | async-done | bytes 1048592 | tf_op jit(solution)/shard_map/all_gather | solution.py:139
  89.8 2.1 convolution_convert_fusion.2
  92.0 0.9 multiply_subtract_fusion.1
  93.0 1.7 concatenate.22
  94.7 1.0 pad_maximum_fusion
  96.0 22.7 %all-gather.15.cloned.1.call-done = bf16[2048,256]{1,0:T(8,128)(2,1)} async-done(((bf16[512,256]{1,0:T(8,128)(2,1)}), bf16[2048,256]{1,0:T(8,128)(2,1)}) %all-gather.15.cloned.1.call-update) | async-done | bytes 1048592 | tf_op jit(solution)/shard_map/all_gather | solution.py:140
  118.6 2.6 convolution_convert_fusion.4
  121.2 1.2 reshape.432
  124.7 0.8 fusion.9
  125.5 0.8 fusion.10
  126.3 1.4 convolution_multiply_fusion.1
  127.8 0.9 fusion.43
  129.0 1.2 reshape.431
  130.8 16.7 %all-gather.13.cloned.1.call-done = bf16[2048,256]{1,0:T(8,128)(2,1)} async-done(((bf16[512,256]{1,0:T(8,128)(2,1)}), bf16[2048,256]{1,0:T(8,128)(2,1)}) %all-gather.13.cloned.1.call-update) | async-done | bytes 1048592 | tf_op jit(solution)/shard_map/all_gather | solution.py:141
  147.4 28.8 %all-gather.21.cloned.1.call-done = bf16[256,2048]{1,0:T(8,128)(2,1)} async-done(((bf16[256,512]{1,0:T(8,128)(2,1)}), bf16[256,2048]{1,0:T(8,128)(2,1)}) %all-gather.21.cloned.1.call-update) | async-done | bytes 1048592 | tf_op jit(solution)/shard_map/all_gather | solution.py:157
  176.3 4.7 convolution_convert_fusion.1
  181.1 27.5 %reduce-scatter.3.cloned.1.call-done = bf16[384,512]{1,0:T(8,128)(2,1)} async-done(((bf16[384,2048]{1,0:T(8,128)(2,1)}), bf16[384,512]{1,0:T(8,128)(2,1)}) %reduce-scatter.3.cloned.1.call-update) | async-done | bytes 393232 | tf_op jit(solution)/shard_map/reduce_scatter | solution.py:160
  208.5 1.8 fusion.12
  212.7 17.5 %all-gather.23.cloned.1.call-done = bf16[384,2048]{1,0:T(8,128)(2,1)} async-done(((bf16[384,512]{1,0:T(8,128)(2,1)}), bf16[384,2048]{1,0:T(8,128)(2,1)}) %all-gather.23.cloned.1.call-update) | async-done | bytes 1572880 | tf_op jit(solution)/shard_map/all_gather | solution.py:166
  230.2 1.8 fusion
  232.0 97.8 %all-gather.25.cloned.1.call-done = bf16[2048,1280]{1,0:T(8,128)(2,1)} async-done(((bf16[512,1280]{1,0:T(8,128)(2,1)}), bf16[2048,1280]{1,0:T(8,128)(2,1)}) %all-gather.25.cloned.1.call-update) | async-done | bytes 5242896 | tf_op jit(solution)/shard_map/all_gather | solution.py:169
  329.8 6.5 %fusion.15 = f32[384,1280]{1,0:T(8,128)} fusion(bf16[2048,1280]{1,0:T(8,128)(2,1)} %all-gather.25.cloned.1.call-done, bf16[384,2048]{1,0:T(8,128)(2,1)} %all-gather.23.cloned.1.call-done, f32[2048]{0:T(1024)S(1)} %copy-done.12, f32[384]{0:T(512)S(1)} %add_rsqrt_fusion), kind=kOutput, calls=%fused_computation.36 | convolution fusion | flops 2016411648 | bytes 8791552 | tf_op jit(solution)/shard_map/dot_general | solution.py:172
  336.4 91.3 %all-gather.27.cloned.1.call-done = bf16[2048,1280]{1,0:T(8,128)(2,1)} async-done(((bf16[512,1280]{1,0:T(8,128)(2,1)}), bf16[2048,1280]{1,0:T(8,128)(2,1)}) %all-gather.27.cloned.1.call-update) | async-done | bytes 5242896 | tf_op jit(solution)/shard_map/all_gather | solution.py:170
  427.7 98.0 %all-gather.29.cloned.1.call-done = bf16[1280,2048]{1,0:T(8,128)(2,1)} async-done(((bf16[1280,512]{1,0:T(8,128)(2,1)}), bf16[1280,2048]{1,0:T(8,128)(2,1)}) %all-gather.29.cloned.1.call-update) | async-done | bytes 5242896 | tf_op jit(solution)/shard_map/all_gather | solution.py:177
  525.6 10.7 %convolution_convert_fusion = bf16[384,2048]{1,0:T(8,128)(2,1)} fusion(bf16[1280,2048]{1,0:T(8,128)(2,1)} %all-gather.29.cloned.1.call-done, bf16[2048,1280]{1,0:T(8,128)(2,1)} %all-gather.27.cloned.1.call-done, f32[384,1280]{1,0:T(8,128)} %fusion.15, bf16[384,2048]{1,0:T(8,128)(2,1)S(1)} %copy-done.3, f32[2048]{0:T(1024)S(1)} %copy-done.12, ...), kind=kOutput, calls=%fused_computation.15 | convolution fusion | flops 4033413120 | bytes 15607296 | tf_op jit(solution)/shard_map/dot_general | solution.py:175
  536.3 26.5 %reduce-scatter.5.cloned.1.call-done = bf16[384,512]{1,0:T(8,128)(2,1)} async-done(((bf16[384,2048]{1,0:T(8,128)(2,1)}), bf16[384,512]{1,0:T(8,128)(2,1)}) %reduce-scatter.5.cloned.1.call-update) | async-done | bytes 393232 | tf_op jit(solution)/shard_map/reduce_scatter | solution.py:180
  562.8 1.8 fusion.17
  (97 shorter events, 12.1 us)
Async XLA Ops:
  6.5 54.3 %copy-start.10 = (f32[2048]{0:T(1024)S(1)}, f32[2048]{0:T(1024)}, u32[]{:S(2)}) copy-start(f32[2048]{0:T(1024)} %param.18) | copy-start | bytes 24580
  6.5 24.7 %all-gather.11.cloned.1.call-start = ((), (), s32[]{:S(2)}) async-start(), calls=%async_computation.2 | async-start | bytes 1966080 | tf_op jit(solution)/shard_map/all_gather | solution.py:134
  7.3 53.6 %all-gather.17.cloned.1.call-start = ((), (), s32[]{:S(2)}) async-start(), calls=%async_computation.5 | async-start | bytes 1310720 | tf_op jit(solution)/shard_map/all_gather | solution.py:138
  8.0 81.8 %all-gather.19.cloned.1.call-start = ((), (), s32[]{:S(2)}) async-start(), calls=%async_computation.6 | async-start | bytes 1310720 | tf_op jit(solution)/shard_map/all_gather | solution.py:139
  8.7 109.9 %all-gather.15.cloned.1.call-start = ((), (), s32[]{:S(2)}) async-start(), calls=%async_computation.4 | async-start | bytes 1310720 | tf_op jit(solution)/shard_map/all_gather | solution.py:140
  9.3 138.1 %all-gather.13.cloned.1.call-start = ((), (), s32[]{:S(2)}) async-start(), calls=%async_computation.3 | async-start | bytes 1310720 | tf_op jit(solution)/shard_map/all_gather | solution.py:141
  9.9 166.4 %all-gather.21.cloned.1.call-start = ((), (), s32[]{:S(2)}) async-start(), calls=%async_computation.7 | async-start | bytes 1310720 | tf_op jit(solution)/shard_map/all_gather | solution.py:157
  10.5 198.1 %reduce-scatter.3.cloned.1.call-start = ((), (), s32[]{:S(2)}) async-start(), calls=%async_computation.8 | async-start | bytes 1966080 | tf_op jit(solution)/shard_map/reduce_scatter | solution.py:160
  31.3 58.6 %copy-start.1 = (bf16[1,384,2048]{2,1,0:T(8,128)(2,1)S(1)}, bf16[1,384,2048]{2,1,0:T(8,128)(2,1)}, u32[]{:S(2)}) copy-start(bf16[1,384,2048]{2,1,0:T(8,128)(2,1)} %all-gather.11.cloned.1.call-done) | copy-start | bytes 4718596
  33.2 58.7 %copy-start.8 = (f32[384]{0:T(512)}, f32[384]{0:T(512)S(1)}, u32[]{:S(2)}) copy-start(f32[384]{0:T(512)S(1)} %add_rsqrt_fusion.1) | copy-start | bytes 4612
  95.9 26.7 %copy-start.5 = (f32[3,128,4,32]{1,0,3,2:T(4,128)S(1)}, f32[3,128,4,32]{1,0,3,2:T(4,128)}, u32[]{:S(2)}) copy-start(f32[3,128,4,32]{1,0,3,2:T(4,128)} %concatenate.22) | copy-start | bytes 589828
  95.9 26.7 %copy-start.6 = (f32[128,4]{0,1:T(4,128)S(1)}, f32[128,4]{0,1:T(4,128)}, u32[]{:S(2)}) copy-start(f32[128,4]{0,1:T(4,128)} %get-tuple-element.231) | copy-start | bytes 6148
  95.9 26.7 %copy-start.7 = (f32[128,4]{0,1:T(4,128)S(1)}, f32[128,4]{0,1:T(4,128)}, u32[]{:S(2)}) copy-start(f32[128,4]{0,1:T(4,128)} %get-tuple-element.229) | copy-start | bytes 6148
  127.8 48.5 %copy-start.2 = (bf16[1,384,2048]{2,1,0:T(8,128)(2,1)S(1)}, bf16[1,384,2048]{2,1,0:T(8,128)(2,1)}, u32[]{:S(2)}) copy-start(bf16[1,384,2048]{2,1,0:T(8,128)(2,1)} %all-gather.11.cloned.1.call-done) | copy-start | bytes 4718596
  127.8 48.5 %copy-start.9 = (f32[384]{0:T(512)S(1)}, f32[384]{0:T(512)}, u32[]{:S(2)}) copy-start(f32[384]{0:T(512)} %copy-done.8) | copy-start | bytes 4612
  127.8 48.5 %copy-start.11 = (f32[2048]{0:T(1024)S(1)}, f32[2048]{0:T(1024)}, u32[]{:S(2)}) copy-start(f32[2048]{0:T(1024)} %param.18) | copy-start | bytes 24580
  130.7 77.8 %copy-start.4 = (bf16[1,384,512]{2,1,0:T(8,128)(2,1)S(1)}, bf16[1,384,512]{2,1,0:T(8,128)(2,1)}, u32[]{:S(2)}) copy-start(bf16[1,384,512]{2,1,0:T(8,128)(2,1)} %param.17) | copy-start | bytes 1179652
  181.0 49.2 %all-gather.23.cloned.1.call-start = ((), (), s32[]{:S(2)}) async-start(), calls=%async_computation.9 | async-start | bytes 1966080 | tf_op jit(solution)/shard_map/all_gather | solution.py:166
  210.4 119.5 %copy-start.12 = (f32[2048]{0:T(1024)S(1)}, f32[2048]{0:T(1024)}, u32[]{:S(2)}) copy-start(f32[2048]{0:T(1024)} %param.26) | copy-start | bytes 24580
  210.4 119.4 %all-gather.25.cloned.1.call-start = ((), (), s32[]{:S(2)}) async-start(), calls=%async_computation.10 | async-start | bytes 6553600 | tf_op jit(solution)/shard_map/all_gather | solution.py:169
  211.1 216.5 %all-gather.27.cloned.1.call-start = ((), (), s32[]{:S(2)}) async-start(), calls=%async_computation.11 | async-start | bytes 6553600 | tf_op jit(solution)/shard_map/all_gather | solution.py:170
  211.7 313.9 %all-gather.29.cloned.1.call-start = ((), (), s32[]{:S(2)}) async-start(), calls=%async_computation.12 | async-start | bytes 6553600 | tf_op jit(solution)/shard_map/all_gather | solution.py:177
  212.5 350.4 %reduce-scatter.5.cloned.1.call-start = ((), (), s32[]{:S(2)}) async-start(), calls=%async_computation.13 | async-start | bytes 1966080 | tf_op jit(solution)/shard_map/reduce_scatter | solution.py:180
  232.0 293.6 %copy-start.3 = (bf16[384,2048]{1,0:T(8,128)(2,1)S(1)}, bf16[384,2048]{1,0:T(8,128)(2,1)}, u32[]{:S(2)}) copy-start(bf16[384,2048]{1,0:T(8,128)(2,1)} %all-gather.23.cloned.1.call-done) | copy-start | bytes 4718596
  336.4 226.4 %copy-start = (bf16[384,512]{1,0:T(8,128)(2,1)S(1)}, bf16[384,512]{1,0:T(8,128)(2,1)}, u32[]{:S(2)}) copy-start(bf16[384,512]{1,0:T(8,128)(2,1)} %fusion.12) | copy-start | bytes 1179652
Sparse Core Ops, SparseCore 0:
  8.9 22.3 all-gather.10
  32.8 27.9 all-gather.16
  62.4 27.3 all-gather.18
  91.3 27.3 all-gather.14
  120.1 27.3 all-gather.12
  148.9 27.3 all-gather.20
  181.1 27.3 reduce-scatter.2
  210.5 19.6 all-gather.22
  231.8 98.0 all-gather.24
  331.3 96.3 all-gather.26
  429.2 96.3 all-gather.28
  536.5 26.3 reduce-scatter.4
where the time goes:
time: 572 us; the launch traced here: 571 us
  waiting for transfers between devices  505 us (88%)
  matrix products  33.9 us (6%)
  between operations  13.9 us (2%)
  other arithmetic  12.9 us (2%)
    all_gather x1, waiting for transfers between devices, on_device(): lax.all_gather(down_weight, 'fs', axis=1, tiled=True)  98 us
    all_gather x1, waiting for transfers between devices, on_device(): lax.all_gather(gate_weight, 'fs', axis=0, tiled=True)  97.8 us
    all_gather x1, waiting for transfers between devices, on_device(): lax.all_gather(up_weight, 'fs', axis=0, tiled=True)  91.3 us
    all_gather x1, waiting for transfers between devices, on_device(): lax.all_gather(merge_weight, 'fs', axis=1, tiled=True)  28.8 us
    all_gather x1, waiting for transfers between devices, on_device(): lax.all_gather(query_weight, 'fs', axis=0, tiled=True)  27.7 us
    reduce_scatter x1, waiting for transfers between devices, on_device(): lax.psum_scatter(merge_term.astype(jnp.bfloat16), 'tp', scatter_dimension...  27.5 us
    reduce_scatter x1, waiting for transfers between devices, on_device(): lax.psum_scatter(down_term.astype(jnp.bfloat16), 'tp', scatter_dimension=...  26.5 us
    all_gather x1, waiting for transfers between devices, on_device(): lax.all_gather(key_weight, 'fs', axis=0, tiled=True)  26.4 us
  transfers between devices with their start and end apart: 12, of which 12 were waited for; matrix products, arithmetic and copies ran while one was open for 6% of the time, Pallas kernels for 0%

commit v1 on v0

--- a/solution.py
+++ b/solution.py
@@ -8,6 +8,19 @@
 group_eps = 1e-05
 rope_base = 10000.0
 highest_precision = lax.Precision.HIGHEST
+
+
+def ring_gather(value, axis, dim):
+    size, index, rows = (lax.axis_size(axis), lax.axis_index(axis), value.shape[dim])
+    right = [(i, (i + 1) % size) for i in range(size)]
+    whole = jnp.zeros((*value.shape[:dim], size * rows, *value.shape[dim + 1 :]), value.dtype)
+    carried = value
+    for step in range(size):
+        source = (index - step) % size
+        whole = lax.dynamic_update_slice_in_dim(whole, carried, source * rows, axis=dim)
+        if step < size - 1:
+            carried = lax.ppermute(carried, axis, right)
+    return whole
 
 
 def rms_scale(values, gain_vector):
@@ -167,7 +180,7 @@
     normed_mid = rms_scale(gathered_mid, middle_gain)
     gate_full, up_full = (
         lax.all_gather(gate_weight, "fs", axis=0, tiled=True),
-        lax.all_gather(up_weight, "fs", axis=0, tiled=True),
+        ring_gather(up_weight, "fs", 0),
     )
     gate_act = jnp.dot(normed_mid, gate_full, preferred_element_type=jnp.float32)
     up_act = jnp.dot(normed_mid, up_full, preferred_element_type=jnp.float32)

time: 572 us -> 528 us (0.923)
  waiting for transfers between devices: 505 us -> 428 us
  starting transfers between devices: 0.61 us -> 29 us
  local copies, waits for them, and re-layouts: 5.47 us -> 12 us
    ppermute x0 -> x3, waiting for transfers between devices: none -> 138 us  [ring_gather(): carried = lax.ppermute(carried, axis, right)]
    all_gather x1, waiting for transfers between devices: 97.8 us -> 0.02 us  [on_device(): lax.all_gather(gate_weight, 'fs', axis=0, tiled=True)]
    all_gather x1 -> x0, waiting for transfers between devices: 91.3 us -> none  [on_device(): lax.all_gather(up_weight, 'fs', axis=0, tiled=True)]
    ppermute x0 -> x3, starting transfers between devices: none -> 28.6 us  [ring_gather(): carried = lax.ppermute(carried, axis, right)]
    all_gather x1, waiting for transfers between devices: 17.5 us -> 0.01 us  [on_device(): gathered_mid = lax.all_gather(middle, 'tp', axis=1, tiled=True)]
    all_gather x1, waiting for transfers between devices: 98 us -> 84.3 us  [on_device(): lax.all_gather(down_weight, 'fs', axis=1, tiled=True)]
    dynamic_update_slice x0 -> x4, local copies, waits for them, and re-layouts: none -> 7.31 us  [ring_gather(): lax.dynamic_update_slice_in_dim(whole, carried, source * rows, axis=dim)]
  transfers between devices with their start and end apart: 12 -> 14, of which waited for: 12 -> 12; matrix products, arithmetic and copies ran while one was open for 6% -> 7% of each run, Pallas kernels for 0% -> 0%
where the time goes in v1:
time: 528 us; the launch traced here: 527 us
  waiting for transfers between devices  428 us (81%)
  matrix products  33.8 us (6%)
  starting transfers between devices  29 us (5%)
  between operations  13.6 us (3%)
  local copies, waits for them, and re-layouts  12 us (2%)
  other arithmetic  10.6 us (2%)
    ppermute x3, waiting for transfers between devices, ring_gather(): carried = lax.ppermute(carried, axis, right)  138 us
    all_gather x1, waiting for transfers between devices, on_device(): lax.all_gather(down_weight, 'fs', axis=1, tiled=True)  84.3 us
    all_gather x1, waiting for transfers between devices, on_device(): lax.all_gather(merge_weight, 'fs', axis=1, tiled=True)  28.8 us
    ppermute x3, starting transfers between devices, ring_gather(): carried = lax.ppermute(carried, axis, right)  28.6 us
    all_gather x1, waiting for transfers between devices, on_device(): lax.all_gather(query_weight, 'fs', axis=0, tiled=True)  27.7 us
    reduce_scatter x1, waiting for transfers between devices, on_device(): lax.psum_scatter(merge_term.astype(jnp.bfloat16), 'tp', scatter_dimension...  27.5 us
    reduce_scatter x1, waiting for transfers between devices, on_device(): lax.psum_scatter(down_term.astype(jnp.bfloat16), 'tp', scatter_dimension=...  26.5 us
    all_gather x1, waiting for transfers between devices, on_device(): lax.all_gather(key_weight, 'fs', axis=0, tiled=True)  26.4 us
  transfers between devices with their start and end apart: 14, of which 12 were waited for; matrix products, arithmetic and copies ran while one was open for 7% of the time, Pallas kernels for 0%

profile of v1, /device:TPU:0, one launch (start us, length us, event | category | flops | bytes accessed | tf_op | source)
XLA Modules:
  0.0 527.1 jit_solution(7453854581385990632)
XLA Ops:
  11.9 19.3 %all-gather.10.cloned.1.call-done = bf16[1,384,2048]{2,1,0:T(8,128)(2,1)} async-done(((bf16[1,384,512]{2,1,0:T(8,128)(2,1)}), bf16[1,384,2048]{2,1,0:T(8,128)(2,1)}) %all-gather.10.cloned.1.call-update) | async-done | bytes 1572880 | tf_op jit(solution)/shard_map/all_gather | solution.py:147
  31.3 1.9 fusion.3
  33.2 27.7 %all-gather.16.cloned.1.call-done = bf16[2048,256]{1,0:T(8,128)(2,1)} async-done(((bf16[512,256]{1,0:T(8,128)(2,1)}), bf16[2048,256]{1,0:T(8,128)(2,1)}) %all-gather.16.cloned.1.call-update) | async-done | bytes 1048592 | tf_op jit(solution)/shard_map/all_gather | solution.py:151
  60.9 2.6 convolution_convert_fusion.3
  63.5 26.4 %all-gather.18.cloned.1.call-done = bf16[2048,256]{1,0:T(8,128)(2,1)} async-done(((bf16[512,256]{1,0:T(8,128)(2,1)}), bf16[2048,256]{1,0:T(8,128)(2,1)}) %all-gather.18.cloned.1.call-update) | async-done | bytes 1048592 | tf_op jit(solution)/shard_map/all_gather | solution.py:152
  89.8 2.1 convolution_convert_fusion.2
  93.0 25.7 %all-gather.14.cloned.1.call-done = bf16[2048,256]{1,0:T(8,128)(2,1)} async-done(((bf16[512,256]{1,0:T(8,128)(2,1)}), bf16[2048,256]{1,0:T(8,128)(2,1)}) %all-gather.14.cloned.1.call-update) | async-done | bytes 1048592 | tf_op jit(solution)/shard_map/all_gather | solution.py:153
  118.6 1.9 convolution_convert_fusion.4
  124.1 0.8 fusion.10
  124.9 1.4 convolution_multiply_fusion.1
  126.3 0.9 fusion.43
  128.5 18.9 %all-gather.12.cloned.1.call-done = bf16[2048,256]{1,0:T(8,128)(2,1)} async-done(((bf16[512,256]{1,0:T(8,128)(2,1)}), bf16[2048,256]{1,0:T(8,128)(2,1)}) %all-gather.12.cloned.1.call-update) | async-done | bytes 1048592 | tf_op jit(solution)/shard_map/all_gather | solution.py:154
  147.5 28.8 %all-gather.20.cloned.1.call-done = bf16[256,2048]{1,0:T(8,128)(2,1)} async-done(((bf16[256,512]{1,0:T(8,128)(2,1)}), bf16[256,2048]{1,0:T(8,128)(2,1)}) %all-gather.20.cloned.1.call-update) | async-done | bytes 1048592 | tf_op jit(solution)/shard_map/all_gather | solution.py:170
  176.3 4.6 convolution_convert_fusion.1
  180.9 27.5 %reduce-scatter.3.cloned.1.call-done = bf16[384,512]{1,0:T(8,128)(2,1)} async-done(((bf16[384,2048]{1,0:T(8,128)(2,1)}), bf16[384,512]{1,0:T(8,128)(2,1)}) %reduce-scatter.3.cloned.1.call-update) | async-done | bytes 393232 | tf_op jit(solution)/shard_map/reduce_scatter | solution.py:173
  208.4 1.8 fusion.12
  211.7 1.6 collective-permute-start
  213.2 30.7 %collective-permute-done = bf16[512,1280]{1,0:T(8,128)(2,1)S(1)} collective-permute-done((bf16[512,1280]{1,0:T(8,128)(2,1)S(1)}, bf16[512,1280]{1,0:T(8,128)(2,1)S(1)}, u32[]{:S(2)}, u32[]{:S(2)}) %collective-permute-start) | collective-permute-done | bytes 1310752 | tf_op jit(solution)/shard_map/ppermute | solution.py:22
  244.1 60.8 %collective-permute-done.1 = bf16[512,1280]{1,0:T(8,128)(2,1)} collective-permute-done((bf16[512,1280]{1,0:T(8,128)(2,1)S(1)}, bf16[512,1280]{1,0:T(8,128)(2,1)}, u32[]{:S(2)}, u32[]{:S(2)}) %collective-permute-start.1) | collective-permute-done | bytes 1310752 | tf_op jit(solution)/shard_map/ppermute | solution.py:22
  304.9 26.9 %collective-permute-start.2 = (bf16[512,1280]{1,0:T(8,128)(2,1)}, bf16[512,1280]{1,0:T(8,128)(2,1)}, u32[]{:S(2)}, u32[]{:S(2)}) collective-permute-start(bf16[512,1280]{1,0:T(8,128)(2,1)} %collective-permute-done.1), channel_id=1, source_target_pairs={{0,4},{4,8},{8,12},{12,0},{1,5},{5,9},{9,13},{13,1},{2,6},{6,10},{... | collective-permute-start | bytes 3932168 | tf_op jit(solution)/shard_map/ppermute | solution.py:22
  331.8 2.6 broadcast_in_dim.30
  334.4 1.2 constant_dynamic-update-slice_fusion.5
  335.7 1.1 constant_dynamic-update-slice_fusion.4
  336.8 2.5 constant_dynamic-update-slice_fusion.3
  339.3 46.3 %collective-permute-done.2 = bf16[512,1280]{1,0:T(8,128)(2,1)} collective-permute-done((bf16[512,1280]{1,0:T(8,128)(2,1)}, bf16[512,1280]{1,0:T(8,128)(2,1)}, u32[]{:S(2)}, u32[]{:S(2)}) %collective-permute-start.2) | collective-permute-done | bytes 1310752 | tf_op jit(solution)/shard_map/ppermute | solution.py:22
  385.6 2.5 constant_dynamic-update-slice_fusion.2
  388.0 1.8 fusion
  389.9 7.3 %fusion.15 = f32[384,1280]{1,0:T(8,128)} fusion(bf16[2048,1280]{1,0:T(8,128)(2,1)} %all-gather.24.cloned.1.call-done, bf16[384,2048]{1,0:T(8,128)(2,1)} %all-gather.22.cloned.1.call-done, f32[2048]{0:T(1024)S(1)} %copy-done.8, f32[384]{0:T(512)S(1)} %add_rsqrt_fusion), kind=kOutput, calls=%fused_computation.36 | convolution fusion | flops 2016411648 | bytes 8791552 | tf_op jit(solution)/shard_map/dot_general | solution.py:185
  397.1 84.3 %all-gather.26.cloned.1.call-done = bf16[1280,2048]{1,0:T(8,128)(2,1)} async-done(((bf16[1280,512]{1,0:T(8,128)(2,1)}), bf16[1280,2048]{1,0:T(8,128)(2,1)}) %all-gather.26.cloned.1.call-update) | async-done | bytes 5242896 | tf_op jit(solution)/shard_map/all_gather | solution.py:190
  481.5 10.7 %convolution_convert_fusion = bf16[384,2048]{1,0:T(8,128)(2,1)} fusion(bf16[1280,2048]{1,0:T(8,128)(2,1)} %all-gather.26.cloned.1.call-done, bf16[2048,1280]{1,0:T(8,128)(2,1)} %constant_dynamic-update-slice_fusion.2, f32[384,1280]{1,0:T(8,128)} %fusion.15, bf16[384,2048]{1,0:T(8,128)(2,1)S(1)} %copy-done.3, f32[2048]{0:T(1024)S(1)} %copy-done.8, ...), kind=kOutput, calls=%fused_computation.15 | convolution fusion | flops 4033413120 | bytes 15607296 | tf_op jit(solution)/shard_map/dot_general | solution.py:188
  492.2 26.5 %reduce-scatter.5.cloned.1.call-done = bf16[384,512]{1,0:T(8,128)(2,1)} async-done(((bf16[384,2048]{1,0:T(8,128)(2,1)}), bf16[384,512]{1,0:T(8,128)(2,1)}) %reduce-scatter.5.cloned.1.call-update) | async-done | bytes 393232 | tf_op jit(solution)/shard_map/reduce_scatter | solution.py:193
  518.7 1.8 fusion.17
  (97 shorter events, 13.2 us)
Async XLA Ops:
  6.5 54.3 %copy-start.7 = (f32[2048]{0:T(1024)S(1)}, f32[2048]{0:T(1024)}, u32[]{:S(2)}) copy-start(f32[2048]{0:T(1024)} %param.18) | copy-start | bytes 24580
  6.5 24.7 %all-gather.10.cloned.1.call-start = ((), (), s32[]{:S(2)}) async-start(), calls=%async_computation.2 | async-start | bytes 1966080 | tf_op jit(solution)/shard_map/all_gather | solution.py:147
  7.3 53.6 %all-gather.16.cloned.1.call-start = ((), (), s32[]{:S(2)}) async-start(), calls=%async_computation.5 | async-start | bytes 1310720 | tf_op jit(solution)/shard_map/all_gather | solution.py:151
  8.0 81.8 %all-gather.18.cloned.1.call-start = ((), (), s32[]{:S(2)}) async-start(), calls=%async_computation.6 | async-start | bytes 1310720 | tf_op jit(solution)/shard_map/all_gather | solution.py:152
  8.7 109.9 %all-gather.14.cloned.1.call-start = ((), (), s32[]{:S(2)}) async-start(), calls=%async_computation.4 | async-start | bytes 1310720 | tf_op jit(solution)/shard_map/all_gather | solution.py:153
  9.3 138.1 %all-gather.12.cloned.1.call-start = ((), (), s32[]{:S(2)}) async-start(), calls=%async_computation.3 | async-start | bytes 1310720 | tf_op jit(solution)/shard_map/all_gather | solution.py:154
  9.9 166.4 %all-gather.20.cloned.1.call-start = ((), (), s32[]{:S(2)}) async-start(), calls=%async_computation.7 | async-start | bytes 1310720 | tf_op jit(solution)/shard_map/all_gather | solution.py:170
  10.5 197.9 %reduce-scatter.3.cloned.1.call-start = ((), (), s32[]{:S(2)}) async-start(), calls=%async_computation.8 | async-start | bytes 1966080 | tf_op jit(solution)/shard_map/reduce_scatter | solution.py:173
  31.3 58.6 %copy-start.1 = (bf16[1,384,2048]{2,1,0:T(8,128)(2,1)S(1)}, bf16[1,384,2048]{2,1,0:T(8,128)(2,1)}, u32[]{:S(2)}) copy-start(bf16[1,384,2048]{2,1,0:T(8,128)(2,1)} %all-gather.10.cloned.1.call-done) | copy-start | bytes 4718596
  121.0 1.2 copy-start.6
  126.3 50.0 %copy-start.2 = (bf16[1,384,2048]{2,1,0:T(8,128)(2,1)S(1)}, bf16[1,384,2048]{2,1,0:T(8,128)(2,1)}, u32[]{:S(2)}) copy-start(bf16[1,384,2048]{2,1,0:T(8,128)(2,1)} %all-gather.10.cloned.1.call-done) | copy-start | bytes 4718596
  128.5 79.9 %copy-start.4 = (bf16[1,384,512]{2,1,0:T(8,128)(2,1)S(1)}, bf16[1,384,512]{2,1,0:T(8,128)(2,1)}, u32[]{:S(2)}) copy-start(bf16[1,384,512]{2,1,0:T(8,128)(2,1)} %param.17) | copy-start | bytes 1179652
  180.9 30.8 %copy-start.5 = (bf16[512,1280]{1,0:T(8,128)(2,1)S(1)}, bf16[512,1280]{1,0:T(8,128)(2,1)}, u32[]{:S(2)}) copy-start(bf16[512,1280]{1,0:T(8,128)(2,1)} %param.28) | copy-start | bytes 3932164
  180.9 207.1 %all-gather.22.cloned.1.call-start = ((), (), s32[]{:S(2)}) async-start(), calls=%async_computation.9 | async-start | bytes 1966080 | tf_op jit(solution)/shard_map/all_gather | solution.py:179
  210.3 179.6 %all-gather.24.cloned.1.call-start = ((), (), s32[]{:S(2)}) async-start(), calls=%async_computation.10 | async-start | bytes 6553600 | tf_op jit(solution)/shard_map/all_gather | solution.py:182
  211.0 270.5 %all-gather.26.cloned.1.call-start = ((), (), s32[]{:S(2)}) async-start(), calls=%async_computation.11 | async-start | bytes 6553600 | tf_op jit(solution)/shard_map/all_gather | solution.py:190
  211.6 307.1 %reduce-scatter.5.cloned.1.call-start = ((), (), s32[]{:S(2)}) async-start(), calls=%async_computation.12 | async-start | bytes 1966080 | tf_op jit(solution)/shard_map/reduce_scatter | solution.py:193
  211.7 32.3 %collective-permute-start = (bf16[512,1280]{1,0:T(8,128)(2,1)S(1)}, bf16[512,1280]{1,0:T(8,128)(2,1)S(1)}, u32[]{:S(2)}, u32[]{:S(2)}) collective-permute-start(bf16[512,1280]{1,0:T(8,128)(2,1)S(1)} %copy-done.5), channel_id=1, source_target_pairs={{0,4},{4,8},{8,12},{12,0},{1,5},{5,9},{9,13},{13,1},{2,6},{6,10},{... | collective-permute-start | bytes 3932168 | tf_op jit(solution)/shard_map/ppermute | solution.py:22
  244.0 60.9 %collective-permute-start.1 = (bf16[512,1280]{1,0:T(8,128)(2,1)S(1)}, bf16[512,1280]{1,0:T(8,128)(2,1)}, u32[]{:S(2)}, u32[]{:S(2)}) collective-permute-start(bf16[512,1280]{1,0:T(8,128)(2,1)S(1)} %collective-permute-done), channel_id=1, source_target_pairs={{0,4},{4,8},{8,12},{12,0},{1,5},{5,9},{9,13},{13,1},{2,6},{6,10},{... | collective-permute-start | bytes 3932168 | tf_op jit(solution)/shard_map/ppermute | solution.py:22
  304.9 80.7 %collective-permute-start.2 = (bf16[512,1280]{1,0:T(8,128)(2,1)}, bf16[512,1280]{1,0:T(8,128)(2,1)}, u32[]{:S(2)}, u32[]{:S(2)}) collective-permute-start(bf16[512,1280]{1,0:T(8,128)(2,1)} %collective-permute-done.1), channel_id=1, source_target_pairs={{0,4},{4,8},{8,12},{12,0},{1,5},{5,9},{9,13},{13,1},{2,6},{6,10},{... | collective-permute-start | bytes 3932168 | tf_op jit(solution)/shard_map/ppermute | solution.py:22
  336.8 53.1 %copy-start.8 = (f32[2048]{0:T(1024)S(1)}, f32[2048]{0:T(1024)}, u32[]{:S(2)}) copy-start(f32[2048]{0:T(1024)} %param.26) | copy-start | bytes 24580
  389.8 91.7 %copy-start.3 = (bf16[384,2048]{1,0:T(8,128)(2,1)S(1)}, bf16[384,2048]{1,0:T(8,128)(2,1)}, u32[]{:S(2)}) copy-start(bf16[384,2048]{1,0:T(8,128)(2,1)} %all-gather.22.cloned.1.call-done) | copy-start | bytes 4718596
  397.1 121.6 %copy-start = (bf16[384,512]{1,0:T(8,128)(2,1)S(1)}, bf16[384,512]{1,0:T(8,128)(2,1)}, u32[]{:S(2)}) copy-start(bf16[384,512]{1,0:T(8,128)(2,1)} %fusion.12) | copy-start | bytes 1179652
Sparse Core Ops, SparseCore 0:
  8.9 22.3 all-gather.9
  32.8 27.9 all-gather.15
  62.4 27.3 all-gather.17
  91.3 27.3 all-gather.13
  120.1 27.3 all-gather.11
  148.9 27.3 all-gather.19
  181.0 27.3 reduce-scatter.2
  210.4 19.6 all-gather.21
  231.7 149.4 all-gather.23
  382.6 98.8 all-gather.25
  492.3 26.3 reduce-scatter.4
